TPU v7x, 32 devices: a whole 2x2x4 slice. The times are simulated.
32 devices in a mesh: gr: 2 (over x), sp: 8 (over z, y), tp: 2 (over core).
Axes of the slice: x: 2, y: 2, z: 4, core: 2. Of those that a mesh axis runs over, the one named last changes fastest.
Arguments:
- tokens: bfloat16 [8, 2048, 2048], P('gr', 'sp'), parts along dimension 0, may hold values from -6 to 6
- new_rows: bfloat16 [8, 2048], P('gr'), parts along dimension 0, may hold values from -6 to 6
- new_query: bfloat16 [8, 1024], P('gr', 'tp'), parts along dimension 0, may hold values from -6 to 6
- norm_gain: bfloat16 [2048], replicated, may hold values from 0.099609375 to 1.8984375
- key_weight: bfloat16 [2048, 1024], P('sp', 'tp'), may hold values from -0.125 to 0.125
- value_weight: bfloat16 [2048, 2048], P('sp', 'tp'), may hold values from -0.125 to 0.125
- input_weight: bfloat16 [2048, 16], replicated, may hold values from -0.125 to 0.125
- forget_weight: bfloat16 [2048, 16], replicated, may hold values from -0.125 to 0.125
- forget_bias: float32 [16], P('tp'), may hold values from 3 to 12
- gate_offsets: float32 [8, 2048, 2, 16], P('gr', 'sp', None, 'tp'), parts along dimension 0, may hold values from -6 to 250, as said below
Outputs:
- cache_keys: bfloat16 [16, 1024, 1024], P(('gr', 'sp'), None, 'tp'), parts along dimension 0
- cache_values: bfloat16 [16, 1024, 2048], P(('gr', 'sp'), None, 'tp'), parts along dimension 0
- cache_weights: float32 [16, 16, 1024], P(('gr', 'sp'), 'tp'), parts along dimension 0
- first_read: bfloat16 [8, 2048], P('gr', 'tp'), parts along dimension 0
There are 2 independent parts, one for each index of `gr`. A program takes and returns all parts, laid end to end along the dimension named above; an argument that names none is the same for every part. Nothing has to cross between parts.
Inputs may be any that keep to these rules, and one draw needn't show every extreme that they name: `gate_offsets`: entry 1 along the third dimension is never positive.
All inputs are finite; a program needn't handle non-finite values.
Results may differ from a plain program's by a relative error of at most 0.012.
The roundings to bfloat16 on the way count: a program that leaves them out, or rounds other values in their place, can miss the bound.
Values may be sent and summed in bfloat16 or wider, within the bound.
No kernel may reach another device: no remote copies, remote signals or barrier semaphores. Data moves between devices by JAX's collectives and lax.ppermute only.
A program may use at most 64 MiB of HBM per device.

v0:
```python
import jax
import jax.numpy as jnp
from jax import lax
from jax.sharding import PartitionSpec as P

EPSILON = 1e-06


def prefix(x, axis, combine, identity):
    devices, index = (lax.axis_size(axis), lax.axis_index(axis))
    everything = lax.all_gather(x, axis)
    start = jnp.broadcast_to(jnp.asarray(identity, x.dtype), x.shape)

    def turn(k, before):
        at = devices - 1 - k
        reached = at > index
        new = combine(before, everything[at])
        return jnp.where(reached, new, before)

    return lax.fori_loop(0, devices, turn, start)


def normed_rows(source, norm_gain):
    widened = source.astype(jnp.float32)
    inverse_rms = lax.rsqrt(jnp.mean(widened * widened, axis=-1, keepdims=True) + EPSILON)
    return (widened * inverse_rms * norm_gain.astype(jnp.float32)).astype(jnp.bfloat16)


def suffix_sums(log_forget):
    flipped = jnp.cumsum(jnp.flip(log_forget, 1), axis=1)
    return jnp.flip(flipped, 1) - log_forget


def add_totals(earlier, following):
    return earlier + following


def partial_read(query_heads, key_heads, value_heads, log_weight, peak_log):
    scores = jnp.einsum("nhd,nshd->nsh", query_heads, key_heads, preferred_element_type=jnp.float32)
    weighted_terms = jnp.exp(log_weight - peak_log[:, None, :]) * scores
    rounded = weighted_terms.astype(jnp.bfloat16)
    numerator = jnp.einsum(
        "nsh,nshd->nhd", rounded, value_heads, preferred_element_type=jnp.float32
    )
    return (numerator, jnp.sum(weighted_terms, axis=1))


def finish_read(numerator, denominator, peak_log, query_heads, key_new, value_new, gate_new):
    peak_new = jnp.maximum(peak_log, gate_new)
    old_part = jnp.exp(peak_log - peak_new)
    own_score = jnp.einsum("nhd,nhd->nh", query_heads, key_new, preferred_element_type=jnp.float32)
    new_part = jnp.exp(gate_new - peak_new) * own_score
    total_value = old_part[..., None] * numerator + new_part[..., None] * value_new.astype(
        jnp.float32
    )
    total_weight = old_part * denominator + new_part
    return total_value / jnp.maximum(jnp.abs(total_weight), 1.0)[..., None]


def per_device(
    tokens,
    new_rows,
    new_query,
    norm_gain,
    key_weight,
    value_weight,
    input_weight,
    forget_weight,
    forget_bias,
    gate_offsets,
):
    seq_count, positions, model_width = tokens.shape
    heads_here = forget_bias.shape[0]
    key_size = key_weight.shape[1] // heads_here
    value_size = value_weight.shape[1] // heads_here
    group_size = lax.axis_size("sp")
    pieces = group_size // seq_count
    sub_rows = positions // pieces
    prompt_rows = seq_count * positions
    normed_all = jnp.concatenate(
        [
            normed_rows(tokens, norm_gain).reshape(prompt_rows, model_width),
            normed_rows(new_rows, norm_gain),
        ],
        axis=0,
    )
    key_sum = jnp.dot(
        normed_all,
        lax.all_gather(key_weight, "sp", axis=0, tiled=True),
        preferred_element_type=jnp.float32,
    )
    value_sum = jnp.dot(
        normed_all,
        lax.all_gather(value_weight, "sp", axis=0, tiled=True),
        preferred_element_type=jnp.float32,
    )
    keys_all = (key_sum * key_size ** (-0.5)).astype(jnp.bfloat16)
    values_all = value_sum.astype(jnp.bfloat16)
    head_start = lax.axis_index("tp") * heads_here
    input_all = lax.dynamic_slice_in_dim(
        jnp.dot(normed_all, input_weight, preferred_element_type=jnp.float32),
        head_start,
        heads_here,
        1,
    )
    forget_all = lax.dynamic_slice_in_dim(
        jnp.dot(normed_all, forget_weight, preferred_element_type=jnp.float32),
        head_start,
        heads_here,
        1,
    )
    key_rows = keys_all[:prompt_rows].reshape(seq_count, positions, heads_here * key_size)
    value_rows = values_all[:prompt_rows].reshape(seq_count, positions, heads_here * value_size)
    input_gate = (
        input_all[:prompt_rows].reshape(seq_count, positions, heads_here) + gate_offsets[:, :, 0, :]
    )
    log_forget = (
        jax.nn.log_sigmoid(
            forget_all[:prompt_rows].reshape(seq_count, positions, heads_here) + forget_bias
        )
        + gate_offsets[:, :, 1, :]
    )
    key_new = keys_all[prompt_rows:].reshape(seq_count, heads_here, key_size)
    value_new = values_all[prompt_rows:].reshape(seq_count, heads_here, value_size)
    gate_new = input_all[prompt_rows:]
    query_all = new_query.reshape(seq_count, heads_here, key_size)
    cache_keys, cache_values = (
        lax.all_to_all(
            key_rows.reshape(seq_count * pieces, sub_rows, heads_here * key_size),
            "sp",
            split_axis=0,
            concat_axis=1,
            tiled=True,
        ),
        lax.all_to_all(
            value_rows.reshape(seq_count * pieces, sub_rows, heads_here * value_size),
            "sp",
            split_axis=0,
            concat_axis=1,
            tiled=True,
        ),
    )
    totals = jnp.sum(log_forget, axis=1)
    tail_sum = prefix(totals, "sp", add_totals, jnp.zeros_like(totals))
    log_weight = input_gate + suffix_sums(log_forget) + tail_sum[:, None, :]
    peak_all = lax.pmax(jnp.max(log_weight, axis=1), "sp")
    numerator, denominator = partial_read(
        query_all,
        key_rows.reshape(seq_count, positions, heads_here, key_size),
        value_rows.reshape(seq_count, positions, heads_here, value_size),
        log_weight,
        peak_all,
    )
    numerator, denominator = lax.psum((numerator, denominator), "sp")
    cache_weight = lax.all_to_all(
        log_weight.reshape(seq_count * pieces, sub_rows, heads_here),
        "sp",
        split_axis=0,
        concat_axis=1,
        tiled=True,
    )
    read_out = finish_read(
        numerator, denominator, peak_all, query_all, key_new, value_new, gate_new
    )
    return (
        cache_keys,
        cache_values,
        jnp.transpose(cache_weight, (0, 2, 1)),
        read_out.reshape(seq_count, heads_here * value_size).astype(jnp.bfloat16),
    )


def solution(mesh):
    return jax.shard_map(
        per_device,
        mesh=mesh,
        in_specs=(
            P("gr", "sp", None),
            P("gr", None),
            P("gr", "tp"),
            P(),
            P("sp", "tp"),
            P("sp", "tp"),
            P(),
            P(),
            P("tp"),
            P("gr", "sp", None, "tp"),
        ),
        out_specs=(
            P(("gr", "sp"), None, "tp"),
            P(("gr", "sp"), None, "tp"),
            P(("gr", "sp"), "tp", None),
            P("gr", "tp"),
        ),
        check_vma=False,
    )
```

profile of v0, /device:TPU:0, one launch (start us, length us, event | category | flops | bytes accessed | tf_op | source)
XLA Modules:
  0.0 284.5 jit_solution(15401344887834810137)
XLA Ops:
  7.2 0.0 copy-start
  7.2 0.0 copy-start.6
  7.2 0.0 all-gather.5.cloned.1.call-start
  7.2 0.7 all-gather.5.cloned.1.call-update
  7.9 0.0 all-gather.7.cloned.1.call-start
  8.0 0.7 all-gather.7.cloned.1.call-update
  8.7 0.7 convert_element_type.38
  9.4 1.0 fusion.8
  10.4 3.3 %fusion = f32[4,256]{1,0:T(4,128)S(1)} fusion(bf16[4,256,2048]{2,1,0:T(8,128)(2,1)} %param.12), kind=kLoop, calls=%fused_computation.3 | loop fusion | flops 6290432 | bytes 4198400 | tf_op jit(solution)/shard_map/reduce_sum | solution.py:25
  13.8 0.1 fusion.10
  13.8 1.0 fusion.2
  14.9 0.0 copy-start.5
  14.9 0.0 copy-start.8
  14.9 0.0 copy-start.9
  14.9 1.3 fusion.27
  16.3 0.6 copy-done.2
  16.9 0.2 fusion.33
  17.0 0.2 rev.7
  17.2 2.3 reduce-window.6
  19.4 0.1 slice.46
  19.5 0.1 copy.30
  19.7 0.1 add_bitcast_fusion
  19.7 0.2 rev.8
  19.9 28.5 %all-gather.1 = f32[8,4,8]{2,1,0:T(4,128)S(1)} all-gather(f32[1,4,8]{2,1,0:T(4,128)S(1)} %bitcast.87), channel_id=2, replica_groups=mesh['gr'=2,'sp'=8,'tp'=2] {'sp'}, dimensions={0}, use_global_device_ids=true | all-gather | bytes 1152 | tf_op jit(solution)/shard_map/all_gather | solution.py:11
  48.4 3.4 %fusion.28 = f32[1028,16]{0,1:T(8,128)S(1)} fusion(bf16[2048,16]{0,1:T(8,128)(2,1)S(1)} %copy-done.9, bf16[4,2048]{1,0:T(4,128)(2,1)S(1)} %fusion.10, bf16[1024,2048]{1,0:T(8,128)(2,1)} %bitcast.77), kind=kOutput, calls=%fused_computation.53 | convolution fusion | flops 75792384 | bytes 4342016 | tf_op jit(solution)/shard_map/dot_general | solution.py:101
  51.8 0.4 while.16
  52.2 0.7 fusion.31
  52.9 3.7 %all-to-all-start.2 = ((f32[8,128,8]{1,2,0:T(8,128)}), f32[8,128,8]{1,2,0:T(8,128)S(1)}, u32[]{:S(2)}, u32[]{:S(2)}) async-start(f32[8,128,8]{1,2,0:T(8,128)} %bitcast.15), calls=%async_computation.2 | async-start | bytes 65536 | tf_op jit(solution)/shard_map/all_to_all | solution.py:155
  56.5 6.3 %all-gather.5.cloned.1.call-done = bf16[2048,512]{1,0:T(8,128)(2,1)} async-done(((bf16[256,512]{1,0:T(8,128)(2,1)}), bf16[2048,512]{1,0:T(8,128)(2,1)}) %all-gather.5.cloned.1.call-update) | async-done | bytes 2097168 | tf_op jit(solution)/shard_map/all_gather | solution.py:89
  62.8 5.2 %fusion.3 = bf16[1028,512]{1,0:T(8,128)(2,1)S(1)} fusion(bf16[2048,512]{1,0:T(8,128)(2,1)} %all-gather.5.cloned.1.call-done, bf16[4,2048]{1,0:T(4,128)(2,1)S(1)} %fusion.10, bf16[1024,2048]{1,0:T(8,128)(2,1)} %bitcast.78), kind=kOutput, calls=%fused_computation.9 | convolution fusion | flops 2165346304 | bytes 7360512 | tf_op jit(solution)/shard_map/dot_general | solution.py:87
  68.0 1.0 copy-done.4
  69.1 1.0 slice.44
  70.1 0.0 all-to-all-done.2
  70.1 3.6 %all-to-all-start = ((bf16[8,128,512]{2,1,0:T(8,128)(2,1)}), bf16[8,128,512]{2,1,0:T(8,128)(2,1)S(1)}, u32[]{:S(2)}, u32[]{:S(2)}) async-start(bf16[8,128,512]{2,1,0:T(8,128)(2,1)} %bitcast.1), calls=%async_computation | async-start | bytes 2097152 | tf_op jit(solution)/shard_map/all_to_all | solution.py:128
  73.7 82.1 %all-gather.7.cloned.1.call-done = bf16[2048,1024]{1,0:T(8,128)(2,1)} async-done(((bf16[256,1024]{1,0:T(8,128)(2,1)}), bf16[2048,1024]{1,0:T(8,128)(2,1)}) %all-gather.7.cloned.1.call-update) | async-done | bytes 4194320 | tf_op jit(solution)/shard_map/all_gather | solution.py:94
  155.8 8.0 %convolution_convert_fusion = bf16[1028,1024]{1,0:T(8,128)(2,1)S(1)} fusion(bf16[2048,1024]{1,0:T(8,128)(2,1)} %all-gather.7.cloned.1.call-done, bf16[4,2048]{1,0:T(4,128)(2,1)S(1)} %fusion.10, bf16[1024,2048]{1,0:T(8,128)(2,1)} %bitcast.79), kind=kOutput, calls=%fused_computation.7 | convolution fusion | flops 4321218560 | bytes 10510336 | tf_op jit(solution)/shard_map/dot_general | solution.py:92
  163.9 1.3 copy-done.3
  165.2 2.2 slice_bitcast_fusion
  167.4 0.0 all-to-all-done
  167.4 4.4 %all-to-all-start.1 = ((bf16[8,128,1024]{2,1,0:T(8,128)(2,1)}), bf16[8,128,1024]{2,1,0:T(8,128)(2,1)}, u32[]{:S(2)}, u32[]{:S(2)}) async-start(bf16[8,128,1024]{2,1,0:T(8,128)(2,1)} %bitcast.3), calls=%async_computation.1 | async-start | bytes 4194304 | tf_op jit(solution)/shard_map/all_to_all | solution.py:135
  171.8 0.1 reshape.80
  171.9 0.1 reshape.95
  172.0 0.1 copy.32
  172.0 48.1 %pmax.7 = f32[4,8]{0,1:T(8,128)S(1)} all-reduce(f32[4,8]{0,1:T(8,128)S(1)} %copy.32), channel_id=1, replica_groups=mesh['gr'=2,'sp'=8,'tp'=2] {'sp'}, use_global_device_ids=true, to_apply=%region_8.9 | all-reduce | flops 32 | bytes 256 | tf_op jit(solution)/shard_map/pmax | solution.py:146
  220.2 0.1 copy.34
  220.3 3.9 %reshape.93 = bf16[4,256,8,64]{3,2,1,0:T(8,128)(2,1)} reshape(bf16[1024,512]{1,0:T(8,128)(2,1)} %slice.44) | data formatting | bytes 2097152 | tf_op jit(solution)/shard_map/reshape;reshape | solution.py:149
  224.2 0.1 reshape.81
  224.2 0.1 fusion.19
  224.3 0.1 copy.48
  224.4 2.2 fusion.4
  226.6 0.9 convert_bitcast_fusion.1
  227.6 0.1 copy.37
  227.7 0.6 copy.53
  228.3 0.4 fusion.6
  228.7 42.6 %all-reduce = (f32[4,8]{0,1:T(8,128)S(1)}, f32[4,8,128]{2,1,0:T(8,128)S(1)}) all-reduce(f32[4,8]{0,1:T(8,128)S(1)} %copy.37, f32[4,8,128]{2,1,0:T(8,128)S(1)} %bitcast.86), channel_id=1, replica_groups=mesh['gr'=2,'sp'=8,'tp'=2] {'sp'}, use_global_device_ids=true, to_apply=%region_11.12 | all-reduce | flops 4128 | bytes 33024 | tf_op jit(solution)/shard_map/psum | solution.py:154
  271.3 0.1 copy.38
  271.4 0.1 copy.33
  271.5 0.1 copy.36
  271.5 0.7 convert_bitcast_fusion
  272.3 0.1 fusion.20
  272.4 0.6 copy.71
  273.0 1.0 copy.81
  273.9 3.1 %copy.82 = bf16[1,1024,1024]{2,1,0:T(8,128)(2,1)} copy(bf16[1,1024,1024]{2,1,0:T(8,128)(2,1)} %bitcast.4) | data formatting | bytes 4194304
  277.0 0.6 copy.83
  (32 shorter events, 0.2 us)
Async XLA Ops:
  7.2 7.7 %copy-start = (bf16[2048,16]{0,1:T(8,128)(2,1)S(1)}, bf16[2048,16]{0,1:T(8,128)(2,1)}, u32[]{:S(2)}) copy-start(bf16[2048,16]{0,1:T(8,128)(2,1)} %param.19) | copy-start | bytes 196612
  7.2 6.6 %copy-start.6 = (bf16[4,2048]{1,0:T(4,128)(2,1)S(1)}, bf16[4,2048]{1,0:T(4,128)(2,1)}, u32[]{:S(2)}) copy-start(bf16[4,2048]{1,0:T(4,128)(2,1)} %param.13) | copy-start | bytes 49156
  7.2 55.6 %all-gather.5.cloned.1.call-start = ((), (), s32[]{:S(2)}) async-start(), calls=%async_computation.3 | async-start | bytes 2359296 | tf_op jit(solution)/shard_map/all_gather | solution.py:89
  7.9 147.9 %all-gather.7.cloned.1.call-start = ((), (), s32[]{:S(2)}) async-start(), calls=%async_computation.4 | async-start | bytes 4718592 | tf_op jit(solution)/shard_map/all_gather | solution.py:94
  9.4 4.5 %copy-start.1 = (bf16[4,256,2048]{2,1,0:T(8,128)(2,1)S(1)}, bf16[4,256,2048]{2,1,0:T(8,128)(2,1)}, u32[]{:S(2)}) copy-start(bf16[4,256,2048]{2,1,0:T(8,128)(2,1)} %param.12) | copy-start | bytes 12582916
  14.9 2.0 copy-start.2
  14.9 1.9 copy-start.5
  14.9 1.9 copy-start.8
  14.9 33.4 %copy-start.9 = (bf16[2048,16]{0,1:T(8,128)(2,1)S(1)}, bf16[2048,16]{0,1:T(8,128)(2,1)}, u32[]{:S(2)}) copy-start(bf16[2048,16]{0,1:T(8,128)(2,1)} %param.18) | copy-start | bytes 196612
  52.9 17.3 %all-to-all-start.2 = ((f32[8,128,8]{1,2,0:T(8,128)}), f32[8,128,8]{1,2,0:T(8,128)S(1)}, u32[]{:S(2)}, u32[]{:S(2)}) async-start(f32[8,128,8]{1,2,0:T(8,128)} %bitcast.15), calls=%async_computation.2 | async-start | bytes 65536 | tf_op jit(solution)/shard_map/all_to_all | solution.py:155
  68.0 1.0 copy-start.4
  70.1 97.3 %all-to-all-start = ((bf16[8,128,512]{2,1,0:T(8,128)(2,1)}), bf16[8,128,512]{2,1,0:T(8,128)(2,1)S(1)}, u32[]{:S(2)}, u32[]{:S(2)}) async-start(bf16[8,128,512]{2,1,0:T(8,128)(2,1)} %bitcast.1), calls=%async_computation | async-start | bytes 2097152 | tf_op jit(solution)/shard_map/all_to_all | solution.py:128
  163.8 1.3 copy-start.3
  165.2 6.6 %copy-start.7 = (bf16[4,512]{1,0:T(4,128)(2,1)S(1)}, bf16[4,512]{1,0:T(4,128)(2,1)}, u32[]{:S(2)}) copy-start(bf16[4,512]{1,0:T(4,128)(2,1)} %param.14) | copy-start | bytes 12292
  167.4 56.8 %slice-start = ((bf16[1028,512]{1,0:T(8,128)(2,1)}), bf16[4,512]{1,0:T(4,128)(2,1)S(1)}, s32[]{:S(2)}) async-start(bf16[1028,512]{1,0:T(8,128)(2,1)} %copy-done.4), calls=%async_computation.5 | async-start | bytes 8192 | tf_op jit(solution)/shard_map/slice | solution.py:123
  167.4 105.6 %all-to-all-start.1 = ((bf16[8,128,1024]{2,1,0:T(8,128)(2,1)}), bf16[8,128,1024]{2,1,0:T(8,128)(2,1)}, u32[]{:S(2)}, u32[]{:S(2)}) async-start(bf16[8,128,1024]{2,1,0:T(8,128)(2,1)} %bitcast.3), calls=%async_computation.1 | async-start | bytes 4194304 | tf_op jit(solution)/shard_map/all_to_all | solution.py:135
Sparse Core Ops, SparseCore 0:
  10.1 52.6 all-gather.4
  64.9 90.8 all-gather.6
where the time goes:
time: 285 us; the launch traced here: 284 us
  blocking collectives  119 us (42%)
  waiting for transfers between devices  89.7 us (31%)
  matrix products  20.6 us (7%)
  local copies, waits for them, and re-layouts  17.4 us (6%)
  between operations  14.2 us (5%)
  starting transfers between devices  11.7 us (4%)
  other arithmetic  11.3 us (4%)
    all_gather x1, waiting for transfers between devices, per_device(): lax.all_gather(value_weight, 'sp', axis=0, tiled=True)  82.1 us
    pmax x1, blocking collectives, per_device(): peak_all = lax.pmax(jnp.max(log_weight, axis=1), 'sp')  48.1 us
    psum x1, blocking collectives, per_device(): numerator, denominator = lax.psum((numerator, denominator), 'sp')  42.6 us
    all_gather x1, blocking collectives, prefix(): everything = lax.all_gather(x, axis)  28.5 us
    unnamed x26, local copies, waits for them, and re-layouts  11.1 us
    dot_general x1, matrix products, per_device(): jnp.dot(normed_all, lax.all_gather(value_weight, 'sp', axis=0, tiled=True...  8.03 us
    all_gather x1, waiting for transfers between devices, per_device(): lax.all_gather(key_weight, 'sp', axis=0, tiled=True)  6.26 us
  transfers between devices with their start and end apart: 5, of which 2 were waited for; matrix products, arithmetic and copies ran while one was open for 15% of the time, Pallas kernels for 0%

commit v1 on v0

v1 whole, which is shorter than its diff:
```python
import functools

import jax
import jax.numpy as jnp
from jax import lax
from jax.experimental import pallas as pl
from jax.experimental.pallas import tpu as pltpu
from jax.sharding import PartitionSpec as P

EPSILON = 1e-06


def normed_rows(source, norm_gain):
    widened = source.astype(jnp.float32)
    inverse_rms = lax.rsqrt(jnp.mean(widened * widened, axis=-1, keepdims=True) + EPSILON)
    return (widened * inverse_rms * norm_gain.astype(jnp.float32)).astype(jnp.bfloat16)


def pick(parts, index):
    out = parts[0]
    for k in range(1, len(parts)):
        out = jnp.where(index == k, parts[k], out)
    return out


def ring(x, axis, size, shift):
    return lax.ppermute(x, axis, [(i, (i + shift) % size) for i in range(size)])


def project_kernel(
    first, key_cols, scale, heads, value_size,
    place, x, w, query, logs, peak, *rest,
):
    if first:
        fresh, keys, values, part, new = rest
    else:
        _, _, before, keys, values, part = rest
    rows = x.shape[0]
    sums = jnp.dot(x[...], w[...], preferred_element_type=jnp.float32)
    k = (sums[:, :key_cols] * scale).astype(jnp.bfloat16)
    v = sums[:, key_cols:].astype(jnp.bfloat16)
    keys[...] = k
    values[...] = v
    scores = lax.dot_general(
        query[...], k, (((1,), (1,)), ((), ())), preferred_element_type=jnp.float32
    )
    terms = jnp.exp(logs[...] - peak[...]) * scores
    top = jnp.dot(terms.astype(jnp.bfloat16), v, preferred_element_type=jnp.float32)
    below = jnp.sum(terms, axis=1, keepdims=True)
    for h in range(heads):
        num = top[h : h + 1, h * value_size : (h + 1) * value_size]
        den = jnp.broadcast_to(below[h : h + 1], (1, value_size))
        if first:
            part[h : h + 1] = num
            part[heads + h : heads + h + 1] = den
        else:
            part[h : h + 1] = before[h : h + 1] + num
            part[heads + h : heads + h + 1] = before[heads + h : heads + h + 1] + den
    if first:
        new[...] = jnp.dot(fresh[...], w[...], preferred_element_type=jnp.float32)


def project(place, x, w, query, logs, peak, extra, total, key_cols, heads, scale):
    first = len(extra) == 1
    rows = x.shape[0]
    value_cols = w.shape[1] - key_cols
    value_size = value_cols // heads
    whole = pl.BlockSpec(memory_space=pltpu.VMEM)
    in_specs = [
        whole,
        whole,
        whole,
        pl.BlockSpec((heads, rows), lambda i, at: (0, at[0])),
        whole,
    ]
    out_shape = [
        jax.ShapeDtypeStruct((total, key_cols), jnp.bfloat16),
        jax.ShapeDtypeStruct((total, value_cols), jnp.bfloat16),
        jax.ShapeDtypeStruct((2 * heads, value_size), jnp.float32),
    ]
    out_specs = [
        pl.BlockSpec((rows, key_cols), lambda i, at: (at[0], 0)),
        pl.BlockSpec((rows, value_cols), lambda i, at: (at[0], 0)),
        whole,
    ]
    aliases = {}
    if first:
        in_specs += [whole]
        out_shape += [jax.ShapeDtypeStruct((extra[0].shape[0], w.shape[1]), jnp.float32)]
        out_specs += [whole]
    else:
        in_specs += [pl.BlockSpec(memory_space=pl.ANY), pl.BlockSpec(memory_space=pl.ANY), whole]
        aliases = {6: 0, 7: 1}
    return pl.pallas_call(
        functools.partial(project_kernel, first, key_cols, scale, heads, value_size),
        out_shape=out_shape,
        grid_spec=pltpu.PrefetchScalarGridSpec(
            num_scalar_prefetch=1, grid=(1,), in_specs=in_specs, out_specs=out_specs
        ),
        input_output_aliases=aliases,
        compiler_params=pltpu.CompilerParams(dimension_semantics=("arbitrary",)),
    )(place, x, w, query, logs, peak, *extra)


def per_device(
    tokens,
    new_rows,
    new_query,
    norm_gain,
    key_weight,
    value_weight,
    input_weight,
    forget_weight,
    forget_bias,
    gate_offsets,
):
    seqs, positions, width = tokens.shape
    heads = forget_bias.shape[0]
    key_cols, value_cols = key_weight.shape[1], value_weight.shape[1]
    key_size, value_size = key_cols // heads, value_cols // heads
    groups, group_size, cores = (lax.axis_size(a) for a in ("gr", "sp", "tp"))
    pieces = group_size // seqs
    sub = positions // pieces
    g, s, t = (lax.axis_index(a) for a in ("gr", "sp", "tp"))
    n, p = s // pieces, s % pieces

    def along(x, shift):
        return lax.ppermute(
            x, "sp",
            [(i, (i // pieces + shift) % seqs * pieces + i % pieces) for i in range(group_size)],
        )

    def across(x, shift):
        return lax.ppermute(
            x, "sp",
            [(i, i // pieces * pieces + (i % pieces + shift) % pieces) for i in range(group_size)],
        )

    depth = key_weight.shape[0]
    share = depth // groups
    own = jnp.concatenate([key_weight, value_weight], axis=1)
    held = {(0, 0): lax.dynamic_slice_in_dim(own, g * share, share, 0)}
    held[1, 0] = along(held[0, 0], 1)
    if seqs > 2:
        held[seqs - 1, 0] = along(held[0, 0], -1)
    for k in range(2, seqs - 1):
        held[k, 0] = along(held[k - 1, 0], 1)
    order = [0, 1, seqs - 1] + list(range(2, seqs - 1))
    for k in order:
        for q in range(1, pieces):
            held[k, q] = across(held[k, q - 1], 1)
    weight = jnp.zeros((width, key_cols + value_cols), jnp.bfloat16)
    for k in order:
        for q in range(pieces):
            base = ((n - k) % seqs * pieces + (p - q) % pieces) * depth
            if (k, q) == (0, 0):
                weight = lax.dynamic_update_slice_in_dim(weight, own, base, 0)
                continue
            part = held[k, q]
            for c in range(groups):
                if c:
                    part = ring(part, "gr", groups, 1)
                weight = lax.dynamic_update_slice_in_dim(
                    weight, part, base + (g - c) % groups * share, 0
                )

    normed = normed_rows(tokens, norm_gain)
    mine = lax.dynamic_slice_in_dim(
        normed.reshape(seqs, pieces, cores, sub // cores, width), t, 1, 2
    )[:, :, 0]
    gathered = [lax.dynamic_index_in_dim(mine, p, 1, keepdims=False)]
    for q in range(1, pieces):
        gathered.append(
            across(lax.dynamic_index_in_dim(mine, (p + q) % pieces, 1, keepdims=False), q)
        )
    bundle = jnp.stack([pick(gathered, (p - q) % pieces) for q in range(pieces)], axis=1)

    rows = normed.reshape(seqs * positions, width)
    fresh_all = normed_rows(new_rows, norm_gain)
    start = t * heads
    gate_weight = jnp.concatenate(
        [
            lax.dynamic_slice_in_dim(input_weight, start, heads, 1),
            lax.dynamic_slice_in_dim(forget_weight, start, heads, 1),
        ],
        axis=1,
    )
    sums = lax.dot_general(
        gate_weight, rows, (((0,), (1,)), ((), ())), preferred_element_type=jnp.float32
    ).reshape(2, heads, seqs, positions)
    offsets = jnp.transpose(gate_offsets, (2, 3, 0, 1))
    input_gate = sums[0] + offsets[0]
    log_forget = jax.nn.log_sigmoid(sums[1] + forget_bias[:, None, None]) + offsets[1]
    later = jnp.flip(jnp.cumsum(jnp.flip(log_forget, 2), axis=2), 2) - log_forget
    local = input_gate + later
    stats = jnp.stack([jnp.sum(log_forget, axis=2), jnp.max(local, axis=2)])
    lines = -(-stats.size // sub)
    line = jnp.pad(stats.reshape(-1), (0, lines * sub - stats.size)).reshape(1, lines, sub)
    send = jnp.concatenate(
        [
            jnp.transpose(local.reshape(heads, seqs * pieces, sub), (1, 0, 2)),
            jnp.broadcast_to(line, (group_size, lines, sub)),
        ],
        axis=1,
    )
    got = lax.all_to_all(send, "sp", split_axis=0, concat_axis=0, tiled=True)
    all_stats = got[:, heads:].reshape(group_size, -1)[:, : stats.size]
    all_stats = all_stats.reshape((group_size,) + stats.shape)
    tails = [jnp.zeros_like(stats[0])]
    for j in range(group_size - 1, 0, -1):
        tails.append(tails[-1] + all_stats[j, 0])
    tails = jnp.stack(tails[::-1])
    tops = jnp.max(tails + all_stats[:, 1], axis=0)
    tail = lax.dynamic_index_in_dim(tails, n, 2, keepdims=False)
    peak = lax.dynamic_index_in_dim(tops, n, 1, keepdims=True)
    logs = jnp.transpose(got[:, :heads] + tail[:, :, None], (1, 0, 2)).reshape(heads, -1)

    fresh = lax.dynamic_slice_in_dim(fresh_all, n, 1, 0)
    query = lax.dynamic_slice_in_dim(new_query, n, 1, 0)
    head_of = lax.broadcasted_iota(jnp.int32, (heads, key_cols), 1) // key_size
    lead = lax.broadcasted_iota(jnp.int32, (heads, key_cols), 0)
    spread = jnp.where(head_of == lead, query, jnp.zeros_like(query))
    fresh_block = jnp.broadcast_to(fresh, (16, width))

    total = group_size * sub
    keys = values = part = new = None
    for k in order:
        block = lax.dynamic_index_in_dim(bundle, (n + k) % seqs, 0, keepdims=False)
        if k:
            block = along(block, k if 2 * k <= seqs else k - seqs)
        shares = [block]
        for c in range(1, cores):
            shares.append(ring(block, "tp", cores, c))
        block = jnp.stack([pick(shares, (t - c) % cores) for c in range(cores)], axis=1)
        block = block.reshape(pieces * sub, width)
        place = ((n - k) % seqs).astype(jnp.int32).reshape(1)
        extra = (fresh_block,) if keys is None else (keys, values, part)
        made = project(
            place, block, weight, spread, logs, peak, extra, total, key_cols, heads,
            key_size ** (-0.5),
        )
        if keys is None:
            keys, values, part, new = made
        else:
            keys, values, part = made

    summed = part
    for q in range(1, pieces):
        summed = summed + across(part, q)
    numerator, denominator = summed[:heads], summed[heads:, :1]
    new = new[:1]
    key_new = (new[:, :key_cols] * key_size ** (-0.5)).astype(jnp.bfloat16)
    value_new = new[:, key_cols:].astype(jnp.bfloat16).astype(jnp.float32)
    gate_new = jnp.dot(fresh, gate_weight[:, :heads], preferred_element_type=jnp.float32)
    gate_new = gate_new.reshape(heads, 1)
    peak_new = jnp.maximum(peak, gate_new)
    old_part = jnp.exp(peak - peak_new)
    own_score = jnp.sum(
        spread.astype(jnp.float32) * key_new.astype(jnp.float32), axis=1, keepdims=True
    )
    new_part = jnp.exp(gate_new - peak_new) * own_score
    above = old_part * numerator + new_part * value_new.reshape(heads, value_size)
    below = old_part * denominator + new_part
    read = (above / jnp.maximum(jnp.abs(below), 1.0)).astype(jnp.bfloat16)
    reads = [read] + [along(read, k) for k in range(1, seqs)]
    out = jnp.stack([pick(reads, (n - k) % seqs) for k in range(seqs)])
    return (
        keys[None],
        values[None],
        logs[None],
        out.reshape(seqs, heads * value_size),
    )


def solution(mesh):
    return jax.shard_map(
        per_device,
        mesh=mesh,
        in_specs=(
            P("gr", "sp", None),
            P("gr", None),
            P("gr", "tp"),
            P(),
            P("sp", "tp"),
            P("sp", "tp"),
            P(),
            P(),
            P("tp"),
            P("gr", "sp", None, "tp"),
        ),
        out_specs=(
            P(("gr", "sp"), None, "tp"),
            P(("gr", "sp"), None, "tp"),
            P(("gr", "sp"), "tp", None),
            P("gr", "tp"),
        ),
        check_vma=False,
    )
```

time: 285 us -> 174 us (0.61)
  blocking collectives: 119 us -> 0 us
  waiting for transfers between devices: 89.7 us -> 61.6 us
  starting transfers between devices: 11.7 us -> 36.1 us
  Pallas kernels: 0 us -> 23.7 us
  matrix products: 20.6 us -> 1.47 us
  local copies, waits for them, and re-layouts: 17.4 us -> 30.9 us
  between operations: 14.2 us -> 1.12 us
  other arithmetic: 11.3 us -> 18.1 us
    all_gather x2 -> x0, waiting for transfers between devices: 88.4 us -> none  [the longest x1 82.1 us: per_device(): lax.all_gather(value_weight, 'sp', axis=0, tiled=True)]
    ppermute x0 -> x26, waiting for transfers between devices: none -> 61.6 us  [the longest x9 32 us: along(): lax.ppermute(x, 'sp', [(i, (i // pieces + shift) % seqs * pieces + i % pi...]
    pmax x1 -> x0, blocking collectives: 48.1 us -> none  [per_device(): peak_all = lax.pmax(jnp.max(log_weight, axis=1), 'sp')]
    psum x1 -> x0, blocking collectives: 42.6 us -> none  [per_device(): numerator, denominator = lax.psum((numerator, denominator), 'sp')]
    ppermute x0 -> x26, starting transfers between devices: none -> 32.7 us  [the longest x9 16.8 us: along(): lax.ppermute(x, 'sp', [(i, (i // pieces + shift) % seqs * pieces + i % pi...]
    all_gather x1 -> x0, blocking collectives: 28.5 us -> none  [prefix(): everything = lax.all_gather(x, axis)]
    pallas_call x0 -> x4, Pallas kernels: none -> 23.7 us  [project(): pl.pallas_call(functools.partial(project_kernel, first, key_cols, scale,...]
    dot_general x6 -> x2, matrix products: 20.6 us -> 1.47 us  [the longest x1 1.18 us: per_device(): lax.dot_general(gate_weight, rows, (((0,), (1,)), ((), ())), preferred_el...]
  transfers between devices with their start and end apart: 5 -> 27, of which waited for: 2 -> 12; matrix products, arithmetic and copies ran while one was open for 15% -> 25% of each run, Pallas kernels for 0% -> 4%
where the time goes in v1:
time: 174 us; the launch traced here: 173 us
  waiting for transfers between devices  61.6 us (35%)
  starting transfers between devices  36.1 us (21%)
  local copies, waits for them, and re-layouts  30.9 us (18%)
  Pallas kernels  23.7 us (14%)
  other arithmetic  18.1 us (10%)
    ppermute x9, waiting for transfers between devices, along(): lax.ppermute(x, 'sp', [(i, (i // pieces + shift) % seqs * pieces + i % pi...  32 us
    pallas_call x4, Pallas kernels, project(): pl.pallas_call(functools.partial(project_kernel, first, key_cols, scale,...  23.7 us
    ppermute x11, waiting for transfers between devices, ring(): return lax.ppermute(x, axis, [(i, (i + shift) % size) for i in range(size)])  19.4 us
    ppermute x9, starting transfers between devices, along(): lax.ppermute(x, 'sp', [(i, (i // pieces + shift) % seqs * pieces + i % pi...  16.8 us
    dynamic_update_slice x14, local copies, waits for them, and re-layouts, per_device(): lax.dynamic_update_slice_in_dim(weight, part, base + (g - c) % groups * s...  12.9 us
    ppermute x6, waiting for transfers between devices, across(): lax.ppermute(x, 'sp', [(i, i // pieces * pieces + (i % pieces + shift) %...  10.2 us
    ppermute x11, starting transfers between devices, ring(): return lax.ppermute(x, axis, [(i, (i + shift) % size) for i in range(size)])  8.62 us
    ppermute x6, starting transfers between devices, across(): lax.ppermute(x, 'sp', [(i, i // pieces * pieces + (i % pieces + shift) %...  7.27 us
  transfers between devices with their start and end apart: 27, of which 12 were waited for; matrix products, arithmetic and copies ran while one was open for 25% of the time, Pallas kernels for 4%

profile of v1, /device:TPU:0, one launch (start us, length us, event | category | flops | bytes accessed | tf_op | source)
XLA Modules:
  0.0 173.0 jit_solution(7395233953140863802)
XLA Ops:
  0.6 1.0 constant_dynamic-update-slice_fusion.1
  1.6 1.1 constant_dynamic-update-slice_fusion
  2.7 0.8 constant_dynamic-slice_fusion.5
  3.5 3.0 %collective-permute-start.3 = (bf16[128,1536]{1,0:T(8,128)(2,1)}, bf16[128,1536]{1,0:T(8,128)(2,1)}, u32[]{:S(2)}, u32[]{:S(2)}) collective-permute-start(bf16[128,1536]{1,0:T(8,128)(2,1)} %constant_dynamic-slice_fusion.5), channel_id=1, source_target_pairs={{0,2},{2,0},{4,6},{6,4},{8,10},{10,8},{12,14},{14,12},{1,3},{3,1},... | collective-permute-start | bytes 1179656 | tf_op jit(solution)/shard_map/ppermute | solution.py:134
  6.5 1.6 collective-permute-start.5
  8.1 2.2 %collective-permute-start.9 = (bf16[128,1536]{1,0:T(8,128)(2,1)}, bf16[128,1536]{1,0:T(8,128)(2,1)S(1)}, u32[]{:S(2)}, u32[]{:S(2)}) collective-permute-start(bf16[128,1536]{1,0:T(8,128)(2,1)} %constant_dynamic-slice_fusion.5), channel_id=1, source_target_pairs={{0,12},{2,14},{4,0},{6,2},{8,4},{10,6},{12,8},{14,10},{1,13},{3,15... | collective-permute-start | bytes 1179656 | tf_op jit(solution)/shard_map/ppermute | solution.py:128
  11.0 3.1 %fusion = f32[4,256]{1,0:T(4,128)S(1)} fusion(bf16[4,256,2048]{2,1,0:T(8,128)(2,1)} %param.10), kind=kLoop, calls=%fused_computation.2 | loop fusion | flops 6290432 | bytes 4198400 | tf_op jit(solution)/shard_map/reduce_sum | solution.py:15
  14.2 3.2 %fusion.2 = bf16[4,256,2048]{2,1,0:T(8,128)(2,1)S(1)} fusion(bf16[4,256,2048]{2,1,0:T(8,128)(2,1)} %param.10, f32[2048]{0:T(1024)S(1)} %convert_element_type.31, f32[4,256]{1,0:T(4,128)S(1)} %add_rsqrt_fusion), kind=kLoop, calls=%fused_computation.4 | loop fusion | flops 8388608 | bytes 8400896 | tf_op jit(solution)/shard_map/convert_element_type | solution.py:16
  17.5 2.0 %copy-done.1 = bf16[4,256,2048]{2,1,0:T(8,128)(2,1)} copy-done((bf16[4,256,2048]{2,1,0:T(8,128)(2,1)}, bf16[4,256,2048]{2,1,0:T(8,128)(2,1)S(1)}, u32[]{:S(2)}) %copy-start.1) | copy-done | bytes 4194328
  19.5 1.2 fusion.13
  21.0 2.3 %reduce-window.6 = f32[8,4,2,128]{3,0,1,2:T(8,128)S(1)} reduce-window(f32[8,4,2,128]{3,0,1,2:T(8,128)S(1)} %copy.149, f32[]{:T(128)} %constant.297.clone.1), window={size=1x1x1x128 pad=0_0x0_0x0_0x127_0}, to_apply=%region_1.2 | reduce-window | flops 1040384 | bytes 65540 | tf_op jit(solution)/shard_map/reduce-window
  24.7 3.4 %all-to-all-start = ((f32[8,9,128]{2,1,0:T(8,128)}), f32[8,9,128]{2,1,0:T(8,128)S(1)}, u32[]{:S(2)}, u32[]{:S(2)}) async-start(f32[8,9,128]{2,1,0:T(8,128)} %copy.153), calls=%async_computation | async-start | bytes 131072 | tf_op jit(solution)/shard_map/all_to_all | solution.py:206
  28.1 1.3 dynamic-slice_bitcast_fusion
  29.4 1.9 %collective-permute-start = (bf16[4,64,2048]{2,1,0:T(8,128)(2,1)S(1)}, bf16[4,64,2048]{2,1,0:T(8,128)(2,1)S(1)}, u32[]{:S(2)}, u32[]{:S(2)}) collective-permute-start(bf16[4,64,2048]{2,1,0:T(8,128)(2,1)S(1)} %dynamic-slice_bitcast_fusion), channel_id=1, source_target_pairs={{0,2},{2,0},{4,6},{6,4},{8,10},{10,8},{12,14},{14,12},{1,3},{3,1},... | collective-permute-start | bytes 3145736 | tf_op jit(solution)/shard_map/ppermute | solution.py:134
  32.2 3.0 %broadcast_in_dim.49 = bf16[2048,1536]{1,0:T(8,128)(2,1)} broadcast(bf16[]{:T(256)} %constant.300.clone.1), dimensions={} | broadcast | bytes 6291458 | tf_op jit(solution)/shard_map/broadcast_in_dim | solution.py:152
  35.2 1.0 constant_dynamic-update-slice_fusion.24
  39.4 1.6 collective-permute-start.4
  41.0 0.7 fusion.22
  42.4 1.8 %constant_dynamic-update-slice_fusion.23 = bf16[2048,1536]{1,0:T(8,128)(2,1)} fusion(bf16[2048,1536]{1,0:T(8,128)(2,1)} %constant_dynamic-update-slice_fusion.24, bf16[128,1536]{1,0:T(8,128)(2,1)} %collective-permute-done.3, s32[]{:T(128)S(6)} %select_n.402), kind=kLoop, calls=%fused_computation.98 | loop fusion | bytes 786436 | tf_op jit(solution)/shard_map/dynamic_update_slice | solution.py:163
  44.1 1.8 %collective-permute-start.13 = (bf16[128,1536]{1,0:T(8,128)(2,1)}, bf16[128,1536]{1,0:T(8,128)(2,1)S(1)}, u32[]{:S(2)}, u32[]{:S(2)}) collective-permute-start(bf16[128,1536]{1,0:T(8,128)(2,1)} %collective-permute-done.5), channel_id=1, source_target_pairs={{0,4},{2,6},{4,8},{6,10},{8,12},{10,14},{12,0},{14,2},{1,5},{3,7},... | collective-permute-start | bytes 1179656 | tf_op jit(solution)/shard_map/ppermute | solution.py:128
  46.0 5.7 %collective-permute-done.4 = bf16[128,1536]{1,0:T(8,128)(2,1)S(1)} collective-permute-done((bf16[128,1536]{1,0:T(8,128)(2,1)}, bf16[128,1536]{1,0:T(8,128)(2,1)S(1)}, u32[]{:S(2)}, u32[]{:S(2)}) %collective-permute-start.4) | collective-permute-done | bytes 393248 | tf_op jit(solution)/shard_map/ppermute | solution.py:27
  51.7 1.5 collective-permute-start.10
  53.2 0.8 constant_dynamic-update-slice_fusion.22
  53.9 1.8 %constant_dynamic-update-slice_fusion.21 = bf16[2048,1536]{1,0:T(8,128)(2,1)} fusion(bf16[2048,1536]{1,0:T(8,128)(2,1)} %constant_dynamic-update-slice_fusion.22, bf16[128,1536]{1,0:T(8,128)(2,1)} %collective-permute-done.5, s32[]{:T(128)S(6)} %select_n.406), kind=kLoop, calls=%fused_computation.96 | loop fusion | bytes 786436 | tf_op jit(solution)/shard_map/dynamic_update_slice | solution.py:163
  55.7 4.4 %collective-permute-done.6 = bf16[128,1536]{1,0:T(8,128)(2,1)S(1)} collective-permute-done((bf16[128,1536]{1,0:T(8,128)(2,1)}, bf16[128,1536]{1,0:T(8,128)(2,1)S(1)}, u32[]{:S(2)}, u32[]{:S(2)}) %collective-permute-start.6) | collective-permute-done | bytes 393248 | tf_op jit(solution)/shard_map/ppermute | solution.py:27
  60.3 3.9 %collective-permute-done.7 = bf16[128,1536]{1,0:T(8,128)(2,1)S(1)} collective-permute-done((bf16[128,1536]{1,0:T(8,128)(2,1)}, bf16[128,1536]{1,0:T(8,128)(2,1)S(1)}, u32[]{:S(2)}, u32[]{:S(2)}) %collective-permute-start.7) | collective-permute-done | bytes 393248 | tf_op jit(solution)/shard_map/ppermute | solution.py:134
  64.1 1.5 collective-permute-start.8
  66.2 0.8 constant_dynamic-update-slice_fusion.20
  67.0 0.8 constant_dynamic-update-slice_fusion.19
  67.7 3.3 %collective-permute-done.11 = bf16[128,1536]{1,0:T(8,128)(2,1)S(1)} collective-permute-done((bf16[128,1536]{1,0:T(8,128)(2,1)S(1)}, bf16[128,1536]{1,0:T(8,128)(2,1)S(1)}, u32[]{:S(2)}, u32[]{:S(2)}) %collective-permute-start.11) | collective-permute-done | bytes 393248 | tf_op jit(solution)/shard_map/ppermute | solution.py:134
  71.0 1.4 collective-permute-start.15
  72.4 1.5 collective-permute-start.12
  73.9 1.4 fusion.4
  75.5 1.3 collective-permute-done.8
  76.8 0.8 constant_dynamic-update-slice_fusion.18
  77.6 0.8 constant_dynamic-update-slice_fusion.17
  78.4 3.4 %collective-permute-start.17 = (bf16[2,64,2048]{2,1,0:T(8,128)(2,1)S(1)}, bf16[2,64,2048]{2,1,0:T(8,128)(2,1)S(1)}, u32[]{:S(2)}, u32[]{:S(2)}) collective-permute-start(bf16[2,64,2048]{2,1,0:T(8,128)(2,1)S(1)} %get-tuple-element.46), channel_id=1, source_target_pairs={{0,12},{2,14},{4,0},{6,2},{8,4},{10,6},{12,8},{14,10},{1,13},{3,15... | collective-permute-start | bytes 1572872 | tf_op jit(solution)/shard_map/ppermute | solution.py:128
  81.8 0.8 constant_dynamic-update-slice_fusion.16
  82.6 0.8 constant_dynamic-update-slice_fusion.15
  83.3 8.0 %collective-permute-done.12 = bf16[128,1536]{1,0:T(8,128)(2,1)S(1)} collective-permute-done((bf16[128,1536]{1,0:T(8,128)(2,1)S(1)}, bf16[128,1536]{1,0:T(8,128)(2,1)S(1)}, u32[]{:S(2)}, u32[]{:S(2)}) %collective-permute-start.12) | collective-permute-done | bytes 393248 | tf_op jit(solution)/shard_map/ppermute | solution.py:27
  91.3 1.4 collective-permute-start.19
  92.8 0.8 constant_dynamic-update-slice_fusion.14
  93.6 0.8 constant_dynamic-update-slice_fusion.13
  94.3 2.4 %collective-permute-start.1 = (bf16[2,64,2048]{2,1,0:T(8,128)(2,1)S(1)}, bf16[2,64,2048]{2,1,0:T(8,128)(2,1)S(1)}, u32[]{:S(2)}, u32[]{:S(2)}) collective-permute-start(bf16[2,64,2048]{2,1,0:T(8,128)(2,1)S(1)} %get-tuple-element.45), channel_id=1, source_target_pairs={{0,8},{2,10},{4,12},{6,14},{8,0},{10,2},{12,4},{14,6},{1,9},{3,11}... | collective-permute-start | bytes 1572872 | tf_op jit(solution)/shard_map/ppermute | solution.py:128
  96.7 1.5 collective-permute-start.16
  98.2 0.8 constant_dynamic-update-slice_fusion.12
  99.0 0.8 constant_dynamic-update-slice_fusion.11
  100.0 1.1 copy.166
  101.1 6.9 %collective-permute-done.19 = bf16[2,64,2048]{2,1,0:T(8,128)(2,1)S(1)} collective-permute-done((bf16[2,64,2048]{2,1,0:T(8,128)(2,1)S(1)}, bf16[2,64,2048]{2,1,0:T(8,128)(2,1)S(1)}, u32[]{:S(2)}, u32[]{:S(2)}) %collective-permute-start.19) | collective-permute-done | bytes 524320 | tf_op jit(solution)/shard_map/ppermute | solution.py:128
  108.0 20.3 %collective-permute-done.1 = bf16[2,64,2048]{2,1,0:T(8,128)(2,1)S(1)} collective-permute-done((bf16[2,64,2048]{2,1,0:T(8,128)(2,1)S(1)}, bf16[2,64,2048]{2,1,0:T(8,128)(2,1)S(1)}, u32[]{:S(2)}, u32[]{:S(2)}) %collective-permute-start.1) | collective-permute-done | bytes 524320 | tf_op jit(solution)/shard_map/ppermute | solution.py:128
  128.4 0.8 constant_dynamic-update-slice_fusion.10.w
  129.8 6.6 %shard_map.129 = (bf16[1024,512]{1,0:T(8,128)(2,1)}, bf16[1024,1024]{1,0:T(8,128)(2,1)}, f32[16,128]{1,0:T(8,128)}, f32[16,1536]{1,0:T(8,128)}) custom-call(s32[1]{0:T(128)} %bitcast.46.place, bf16[256,2048]{1,0:T(8,128)(2,1)} %bitcast.178, bf16[2048,1536]{1,0:T(8,128)(2,1)} %constant_dynamic-update-slice_fusion.10.w, bf16[8,512]{1,0:T(8,128)(2,1)} %fusion.24.query, ...), custom_call_target="tpu_custom_call" | custom-call | tf_op jit(solution)/shard_map/pallas_call | solution.py:94
  136.4 0.7 convert_convert_fusion
  137.1 0.8 fusion.35
  138.1 1.1 copy.165
  139.4 1.1 copy.164
  140.5 1.1 pad_maximum_fusion
  141.6 5.7 %shard_map.130 = (bf16[1024,512]{1,0:T(8,128)(2,1)}, bf16[1024,1024]{1,0:T(8,128)(2,1)}, f32[16,128]{1,0:T(8,128)}) custom-call(s32[1]{0:T(128)} %bitcast.41.place, bf16[256,2048]{1,0:T(8,128)(2,1)} %bitcast.175, bf16[2048,1536]{1,0:T(8,128)(2,1)} %constant_dynamic-update-slice_fusion.10.w, ...), custom_call_target="tpu_custom_call", output_to_operand_aliasing={{0}: (6, {}), {1}: (7, {})} | custom-call | tf_op jit(solution)/shard_map/pallas_call | solution.py:94
  147.3 5.7 %shard_map.131 = (bf16[1024,512]{1,0:T(8,128)(2,1)}, bf16[1024,1024]{1,0:T(8,128)(2,1)}, f32[16,128]{1,0:T(8,128)}) custom-call(s32[1]{0:T(128)} %bitcast.35.place, bf16[256,2048]{1,0:T(8,128)(2,1)} %bitcast.176, bf16[2048,1536]{1,0:T(8,128)(2,1)} %constant_dynamic-update-slice_fusion.10.w, ...), custom_call_target="tpu_custom_call", output_to_operand_aliasing={{0}: (6, {}), {1}: (7, {})} | custom-call | tf_op jit(solution)/shard_map/pallas_call | solution.py:94
  153.0 5.7 %shard_map.132 = (bf16[1024,512]{1,0:T(8,128)(2,1)}, bf16[1024,1024]{1,0:T(8,128)(2,1)}, f32[16,128]{1,0:T(8,128)}) custom-call(s32[1]{0:T(128)} %bitcast.place, bf16[256,2048]{1,0:T(8,128)(2,1)} %bitcast.177, bf16[2048,1536]{1,0:T(8,128)(2,1)} %constant_dynamic-update-slice_fusion.10.w, ...), custom_call_target="tpu_custom_call", output_to_operand_aliasing={{0}: (6, {}), {1}: (7, {})} | custom-call | tf_op jit(solution)/shard_map/pallas_call | solution.py:94
  159.5 3.1 %collective-permute-done.22 = f32[16,128]{1,0:T(8,128)S(1)} collective-permute-done((f32[16,128]{1,0:T(8,128)}, f32[16,128]{1,0:T(8,128)S(1)}, u32[]{:S(2)}, u32[]{:S(2)}) %collective-permute-start.22) | collective-permute-done | bytes 8224 | tf_op jit(solution)/shard_map/ppermute | solution.py:134
  163.7 3.3 %collective-permute-start.23 = (bf16[8,128]{1,0:T(8,128)(2,1)S(1)}, bf16[8,128]{1,0:T(8,128)(2,1)S(1)}, u32[]{:S(2)}, u32[]{:S(2)}) collective-permute-start(bf16[8,128]{1,0:T(8,128)(2,1)S(1)} %fusion.38), channel_id=1, source_target_pairs={{0,12},{2,14},{4,0},{6,2},{8,4},{10,6},{12,8},{14,10},{1,13},{3,15... | collective-permute-start | bytes 6152 | tf_op jit(solution)/shard_map/ppermute | solution.py:128
  168.2 3.2 %collective-permute-done.24 = bf16[8,128]{1,0:T(8,128)(2,1)S(1)} collective-permute-done((bf16[8,128]{1,0:T(8,128)(2,1)S(1)}, bf16[8,128]{1,0:T(8,128)(2,1)S(1)}, u32[]{:S(2)}, u32[]{:S(2)}) %collective-permute-start.24) | collective-permute-done | bytes 2080 | tf_op jit(solution)/shard_map/ppermute | solution.py:128
  171.4 0.9 collective-permute-done.25
  (118 shorter events, 13.1 us)
Async XLA Ops:
  0.6 31.5 %copy-start = (bf16[4,512]{1,0:T(4,128)(2,1)S(1)}, bf16[4,512]{1,0:T(4,128)(2,1)}, u32[]{:S(2)}) copy-start(bf16[4,512]{1,0:T(4,128)(2,1)} %param.12) | copy-start | bytes 12292
  3.5 35.9 %collective-permute-start.3 = (bf16[128,1536]{1,0:T(8,128)(2,1)}, bf16[128,1536]{1,0:T(8,128)(2,1)}, u32[]{:S(2)}, u32[]{:S(2)}) collective-permute-start(bf16[128,1536]{1,0:T(8,128)(2,1)} %constant_dynamic-slice_fusion.5), channel_id=1, source_target_pairs={{0,2},{2,0},{4,6},{6,4},{8,10},{10,8},{12,14},{14,12},{1,3},{3,1},... | collective-permute-start | bytes 1179656 | tf_op jit(solution)/shard_map/ppermute | solution.py:134
  6.5 35.2 %collective-permute-start.5 = (bf16[128,1536]{1,0:T(8,128)(2,1)}, bf16[128,1536]{1,0:T(8,128)(2,1)}, u32[]{:S(2)}, u32[]{:S(2)}) collective-permute-start(bf16[128,1536]{1,0:T(8,128)(2,1)} %constant_dynamic-slice_fusion.5), channel_id=1, source_target_pairs={{0,4},{2,6},{4,8},{6,10},{8,12},{10,14},{12,0},{14,2},{1,5},{3,7},... | collective-permute-start | bytes 1179656 | tf_op jit(solution)/shard_map/ppermute | solution.py:128
  8.1 36.1 %collective-permute-start.9 = (bf16[128,1536]{1,0:T(8,128)(2,1)}, bf16[128,1536]{1,0:T(8,128)(2,1)S(1)}, u32[]{:S(2)}, u32[]{:S(2)}) collective-permute-start(bf16[128,1536]{1,0:T(8,128)(2,1)} %constant_dynamic-slice_fusion.5), channel_id=1, source_target_pairs={{0,12},{2,14},{4,0},{6,2},{8,4},{10,6},{12,8},{14,10},{1,13},{3,15... | collective-permute-start | bytes 1179656 | tf_op jit(solution)/shard_map/ppermute | solution.py:128
  11.0 6.4 %copy-start.5 = (bf16[2048,16]{0,1:T(8,128)(2,1)S(1)}, bf16[2048,16]{0,1:T(8,128)(2,1)}, u32[]{:S(2)}) copy-start(bf16[2048,16]{0,1:T(8,128)(2,1)} %param.17) | copy-start | bytes 196612
  11.0 6.4 %copy-start.6 = (bf16[2048,16]{0,1:T(8,128)(2,1)S(1)}, bf16[2048,16]{0,1:T(8,128)(2,1)}, u32[]{:S(2)}) copy-start(bf16[2048,16]{0,1:T(8,128)(2,1)} %param.16) | copy-start | bytes 196612
  14.1 6.5 %copy-start.4 = (f32[4,256,2,8]{1,3,2,0:T(8,128)S(1)}, f32[4,256,2,8]{1,3,2,0:T(8,128)}, u32[]{:S(2)}) copy-start(f32[4,256,2,8]{1,3,2,0:T(8,128)} %param.19) | copy-start | bytes 196612
  14.1 6.6 %copy-start.7 = (f32[8]{0:T(128)S(1)}, f32[8]{0:T(128)}, u32[]{:S(2)}) copy-start(f32[8]{0:T(128)} %param.18) | copy-start | bytes 100
  14.2 17.2 %copy-start.3 = (bf16[4,2048]{1,0:T(4,128)(2,1)S(1)}, bf16[4,2048]{1,0:T(4,128)(2,1)}, u32[]{:S(2)}) copy-start(bf16[4,2048]{1,0:T(4,128)(2,1)} %param.11) | copy-start | bytes 49156
  17.4 2.0 %copy-start.1 = (bf16[4,256,2048]{2,1,0:T(8,128)(2,1)}, bf16[4,256,2048]{2,1,0:T(8,128)(2,1)S(1)}, u32[]{:S(2)}) copy-start(bf16[4,256,2048]{2,1,0:T(8,128)(2,1)S(1)} %fusion.2) | copy-start | bytes 12582916
  24.7 12.8 %all-to-all-start = ((f32[8,9,128]{2,1,0:T(8,128)}), f32[8,9,128]{2,1,0:T(8,128)S(1)}, u32[]{:S(2)}, u32[]{:S(2)}) async-start(f32[8,9,128]{2,1,0:T(8,128)} %copy.153), calls=%async_computation | async-start | bytes 131072 | tf_op jit(solution)/shard_map/all_to_all | solution.py:206
  29.4 43.0 %collective-permute-start = (bf16[4,64,2048]{2,1,0:T(8,128)(2,1)S(1)}, bf16[4,64,2048]{2,1,0:T(8,128)(2,1)S(1)}, u32[]{:S(2)}, u32[]{:S(2)}) collective-permute-start(bf16[4,64,2048]{2,1,0:T(8,128)(2,1)S(1)} %dynamic-slice_bitcast_fusion), channel_id=1, source_target_pairs={{0,2},{2,0},{4,6},{6,4},{8,10},{10,8},{12,14},{14,12},{1,3},{3,1},... | collective-permute-start | bytes 3145736 | tf_op jit(solution)/shard_map/ppermute | solution.py:134
  39.4 12.3 %collective-permute-start.4 = (bf16[128,1536]{1,0:T(8,128)(2,1)}, bf16[128,1536]{1,0:T(8,128)(2,1)S(1)}, u32[]{:S(2)}, u32[]{:S(2)}) collective-permute-start(bf16[128,1536]{1,0:T(8,128)(2,1)} %collective-permute-done.3), channel_id=1, source_target_pairs={{0,16},{16,0},{1,17},{17,1},{2,18},{18,2},{3,19},{19,3},{4,20},{20... | collective-permute-start | bytes 1179656 | tf_op jit(solution)/shard_map/ppermute | solution.py:27
  41.7 18.4 %collective-permute-start.6 = (bf16[128,1536]{1,0:T(8,128)(2,1)}, bf16[128,1536]{1,0:T(8,128)(2,1)S(1)}, u32[]{:S(2)}, u32[]{:S(2)}) collective-permute-start(bf16[128,1536]{1,0:T(8,128)(2,1)} %collective-permute-done.5), channel_id=1, source_target_pairs={{0,16},{16,0},{1,17},{17,1},{2,18},{18,2},{3,19},{19,3},{4,20},{20... | collective-permute-start | bytes 1179656 | tf_op jit(solution)/shard_map/ppermute | solution.py:27
  42.2 21.9 %collective-permute-start.7 = (bf16[128,1536]{1,0:T(8,128)(2,1)}, bf16[128,1536]{1,0:T(8,128)(2,1)S(1)}, u32[]{:S(2)}, u32[]{:S(2)}) collective-permute-start(bf16[128,1536]{1,0:T(8,128)(2,1)} %collective-permute-done.5), channel_id=1, source_target_pairs={{0,2},{2,0},{4,6},{6,4},{8,10},{10,8},{12,14},{14,12},{1,3},{3,1},... | collective-permute-start | bytes 1179656 | tf_op jit(solution)/shard_map/ppermute | solution.py:134
  44.1 21.5 %collective-permute-start.13 = (bf16[128,1536]{1,0:T(8,128)(2,1)}, bf16[128,1536]{1,0:T(8,128)(2,1)S(1)}, u32[]{:S(2)}, u32[]{:S(2)}) collective-permute-start(bf16[128,1536]{1,0:T(8,128)(2,1)} %collective-permute-done.5), channel_id=1, source_target_pairs={{0,4},{2,6},{4,8},{6,10},{8,12},{10,14},{12,0},{14,2},{1,5},{3,7},... | collective-permute-start | bytes 1179656 | tf_op jit(solution)/shard_map/ppermute | solution.py:128
  51.7 26.7 %collective-permute-start.10 = (bf16[128,1536]{1,0:T(8,128)(2,1)S(1)}, bf16[128,1536]{1,0:T(8,128)(2,1)S(1)}, u32[]{:S(2)}, u32[]{:S(2)}) collective-permute-start(bf16[128,1536]{1,0:T(8,128)(2,1)S(1)} %collective-permute-done.9), channel_id=1, source_target_pairs={{0,16},{16,0},{1,17},{17,1},{2,18},{18,2},{3,19},{19,3},{4,20},{20... | collective-permute-start | bytes 1179656 | tf_op jit(solution)/shard_map/ppermute | solution.py:27
  60.1 10.9 %collective-permute-start.11 = (bf16[128,1536]{1,0:T(8,128)(2,1)S(1)}, bf16[128,1536]{1,0:T(8,128)(2,1)S(1)}, u32[]{:S(2)}, u32[]{:S(2)}) collective-permute-start(bf16[128,1536]{1,0:T(8,128)(2,1)S(1)} %collective-permute-done.9), channel_id=1, source_target_pairs={{0,2},{2,0},{4,6},{6,4},{8,10},{10,8},{12,14},{14,12},{1,3},{3,1},... | collective-permute-start | bytes 1179656 | tf_op jit(solution)/shard_map/ppermute | solution.py:134
  64.1 12.7 %collective-permute-start.8 = (bf16[128,1536]{1,0:T(8,128)(2,1)S(1)}, bf16[128,1536]{1,0:T(8,128)(2,1)S(1)}, u32[]{:S(2)}, u32[]{:S(2)}) collective-permute-start(bf16[128,1536]{1,0:T(8,128)(2,1)S(1)} %collective-permute-done.7), channel_id=1, source_target_pairs={{0,16},{16,0},{1,17},{17,1},{2,18},{18,2},{3,19},{19,3},{4,20},{20... | collective-permute-start | bytes 1179656 | tf_op jit(solution)/shard_map/ppermute | solution.py:27
  65.6 28.7 %collective-permute-start.14 = (bf16[128,1536]{1,0:T(8,128)(2,1)S(1)}, bf16[128,1536]{1,0:T(8,128)(2,1)S(1)}, u32[]{:S(2)}, u32[]{:S(2)}) collective-permute-start(bf16[128,1536]{1,0:T(8,128)(2,1)S(1)} %collective-permute-done.13), channel_id=1, source_target_pairs={{0,16},{16,0},{1,17},{17,1},{2,18},{18,2},{3,19},{19,3},{4,20},{20... | collective-permute-start | bytes 1179656 | tf_op jit(solution)/shard_map/ppermute | solution.py:27
  71.0 25.7 %collective-permute-start.15 = (bf16[128,1536]{1,0:T(8,128)(2,1)S(1)}, bf16[128,1536]{1,0:T(8,128)(2,1)S(1)}, u32[]{:S(2)}, u32[]{:S(2)}) collective-permute-start(bf16[128,1536]{1,0:T(8,128)(2,1)S(1)} %collective-permute-done.13), channel_id=1, source_target_pairs={{0,2},{2,0},{4,6},{6,4},{8,10},{10,8},{12,14},{14,12},{1,3},{3,1},... | collective-permute-start | bytes 1179656 | tf_op jit(solution)/shard_map/ppermute | solution.py:134
  72.4 18.9 %collective-permute-start.12 = (bf16[128,1536]{1,0:T(8,128)(2,1)S(1)}, bf16[128,1536]{1,0:T(8,128)(2,1)S(1)}, u32[]{:S(2)}, u32[]{:S(2)}) collective-permute-start(bf16[128,1536]{1,0:T(8,128)(2,1)S(1)} %collective-permute-done.11), channel_id=1, source_target_pairs={{0,16},{16,0},{1,17},{17,1},{2,18},{18,2},{3,19},{19,3},{4,20},{20... | collective-permute-start | bytes 1179656 | tf_op jit(solution)/shard_map/ppermute | solution.py:27
  76.8 23.0 %collective-permute-start.21 = (bf16[2,64,2048]{2,1,0:T(8,128)(2,1)S(1)}, bf16[2,64,2048]{2,1,0:T(8,128)(2,1)S(1)}, u32[]{:S(2)}, u32[]{:S(2)}) collective-permute-start(bf16[2,64,2048]{2,1,0:T(8,128)(2,1)S(1)} %get-tuple-element.44), channel_id=1, source_target_pairs={{0,1},{1,0},{2,3},{3,2},{4,5},{5,4},{6,7},{7,6},{8,9},{9,8},{10,11... | collective-permute-start | bytes 1572872 | tf_op jit(solution)/shard_map/ppermute | solution.py:27
  78.4 22.7 %collective-permute-start.17 = (bf16[2,64,2048]{2,1,0:T(8,128)(2,1)S(1)}, bf16[2,64,2048]{2,1,0:T(8,128)(2,1)S(1)}, u32[]{:S(2)}, u32[]{:S(2)}) collective-permute-start(bf16[2,64,2048]{2,1,0:T(8,128)(2,1)S(1)} %get-tuple-element.46), channel_id=1, source_target_pairs={{0,12},{2,14},{4,0},{6,2},{8,4},{10,6},{12,8},{14,10},{1,13},{3,15... | collective-permute-start | bytes 1572872 | tf_op jit(solution)/shard_map/ppermute | solution.py:128
  91.3 16.7 %collective-permute-start.19 = (bf16[2,64,2048]{2,1,0:T(8,128)(2,1)S(1)}, bf16[2,64,2048]{2,1,0:T(8,128)(2,1)S(1)}, u32[]{:S(2)}, u32[]{:S(2)}) collective-permute-start(bf16[2,64,2048]{2,1,0:T(8,128)(2,1)S(1)} %get-tuple-element.47), channel_id=1, source_target_pairs={{0,4},{2,6},{4,8},{6,10},{8,12},{10,14},{12,0},{14,2},{1,5},{3,7},... | collective-permute-start | bytes 1572872 | tf_op jit(solution)/shard_map/ppermute | solution.py:128
  94.3 34.0 %collective-permute-start.1 = (bf16[2,64,2048]{2,1,0:T(8,128)(2,1)S(1)}, bf16[2,64,2048]{2,1,0:T(8,128)(2,1)S(1)}, u32[]{:S(2)}, u32[]{:S(2)}) collective-permute-start(bf16[2,64,2048]{2,1,0:T(8,128)(2,1)S(1)} %get-tuple-element.45), channel_id=1, source_target_pairs={{0,8},{2,10},{4,12},{6,14},{8,0},{10,2},{12,4},{14,6},{1,9},{3,11}... | collective-permute-start | bytes 1572872 | tf_op jit(solution)/shard_map/ppermute | solution.py:128
  96.7 31.6 %collective-permute-start.16 = (bf16[128,1536]{1,0:T(8,128)(2,1)S(1)}, bf16[128,1536]{1,0:T(8,128)(2,1)S(1)}, u32[]{:S(2)}, u32[]{:S(2)}) collective-permute-start(bf16[128,1536]{1,0:T(8,128)(2,1)S(1)} %collective-permute-done.15), channel_id=1, source_target_pairs={{0,16},{16,0},{1,17},{17,1},{2,18},{18,2},{3,19},{19,3},{4,20},{20... | collective-permute-start | bytes 1179656 | tf_op jit(solution)/shard_map/ppermute | solution.py:27
  101.1 36.8 %collective-permute-start.18 = (bf16[2,64,2048]{2,1,0:T(8,128)(2,1)S(1)}, bf16[2,64,2048]{2,1,0:T(8,128)(2,1)S(1)}, u32[]{:S(2)}, u32[]{:S(2)}) collective-permute-start(bf16[2,64,2048]{2,1,0:T(8,128)(2,1)S(1)} %collective-permute-done.17), channel_id=1, source_target_pairs={{0,1},{1,0},{2,3},{3,2},{4,5},{5,4},{6,7},{7,6},{8,9},{9,8},{10,11... | collective-permute-start | bytes 1572872 | tf_op jit(solution)/shard_map/ppermute | solution.py:27
  108.0 29.9 %collective-permute-start.20 = (bf16[2,64,2048]{2,1,0:T(8,128)(2,1)S(1)}, bf16[2,64,2048]{2,1,0:T(8,128)(2,1)S(1)}, u32[]{:S(2)}, u32[]{:S(2)}) collective-permute-start(bf16[2,64,2048]{2,1,0:T(8,128)(2,1)S(1)} %collective-permute-done.19), channel_id=1, source_target_pairs={{0,1},{1,0},{2,3},{3,2},{4,5},{5,4},{6,7},{7,6},{8,9},{9,8},{10,11... | collective-permute-start | bytes 1572872 | tf_op jit(solution)/shard_map/ppermute | solution.py:27
  128.4 12.1 %collective-permute-start.2 = (bf16[2,64,2048]{2,1,0:T(8,128)(2,1)S(1)}, bf16[2,64,2048]{2,1,0:T(8,128)(2,1)S(1)}, u32[]{:S(2)}, u32[]{:S(2)}) collective-permute-start(bf16[2,64,2048]{2,1,0:T(8,128)(2,1)S(1)} %collective-permute-done.1), channel_id=1, source_target_pairs={{0,1},{1,0},{2,3},{3,2},{4,5},{5,4},{6,7},{7,6},{8,9},{9,8},{10,11... | collective-permute-start | bytes 1572872 | tf_op jit(solution)/shard_map/ppermute | solution.py:27
  153.0 10.3 %copy-start.2 = (f32[8,1]{1,0:T(8,128)S(1)}, f32[8,1]{1,0:T(8,128)}, u32[]{:S(2)}) copy-start(f32[8,1]{1,0:T(8,128)} %copy.172.peak) | copy-start | bytes 100
  158.7 3.9 %collective-permute-start.22 = (f32[16,128]{1,0:T(8,128)}, f32[16,128]{1,0:T(8,128)S(1)}, u32[]{:S(2)}, u32[]{:S(2)}) collective-permute-start(f32[16,128]{1,0:T(8,128)} %get-tuple-element.28), channel_id=1, source_target_pairs={{0,2},{2,0},{4,6},{6,4},{8,10},{10,8},{12,14},{14,12},{1,3},{3,1},... | collective-permute-start | bytes 24584 | tf_op jit(solution)/shard_map/ppermute | solution.py:134
  163.7 4.6 %collective-permute-start.23 = (bf16[8,128]{1,0:T(8,128)(2,1)S(1)}, bf16[8,128]{1,0:T(8,128)(2,1)S(1)}, u32[]{:S(2)}, u32[]{:S(2)}) collective-permute-start(bf16[8,128]{1,0:T(8,128)(2,1)S(1)} %fusion.38), channel_id=1, source_target_pairs={{0,12},{2,14},{4,0},{6,2},{8,4},{10,6},{12,8},{14,10},{1,13},{3,15... | collective-permute-start | bytes 6152 | tf_op jit(solution)/shard_map/ppermute | solution.py:128
  166.9 4.5 %collective-permute-start.24 = (bf16[8,128]{1,0:T(8,128)(2,1)S(1)}, bf16[8,128]{1,0:T(8,128)(2,1)S(1)}, u32[]{:S(2)}, u32[]{:S(2)}) collective-permute-start(bf16[8,128]{1,0:T(8,128)(2,1)S(1)} %fusion.38), channel_id=1, source_target_pairs={{0,8},{2,10},{4,12},{6,14},{8,0},{10,2},{12,4},{14,6},{1,9},{3,11}... | collective-permute-start | bytes 6152 | tf_op jit(solution)/shard_map/ppermute | solution.py:128
  166.9 5.4 %collective-permute-start.25 = (bf16[8,128]{1,0:T(8,128)(2,1)S(1)}, bf16[8,128]{1,0:T(8,128)(2,1)S(1)}, u32[]{:S(2)}, u32[]{:S(2)}) collective-permute-start(bf16[8,128]{1,0:T(8,128)(2,1)S(1)} %fusion.38), channel_id=1, source_target_pairs={{0,4},{2,6},{4,8},{6,10},{8,12},{10,14},{12,0},{14,2},{1,5},{3,7},... | collective-permute-start | bytes 6152 | tf_op jit(solution)/shard_map/ppermute | solution.py:128
